TPU v7x, 32 devices: a whole 2x2x4 slice. The times are simulated.
32 devices in a mesh: sp: 8 (over z, y), tp: 4 (over x, core).
Axes of the slice: x: 2, y: 2, z: 4, core: 2. Of those that a mesh axis runs over, the one named last changes fastest.
Arguments:
- tokens: bfloat16 [2048, 2048], P('sp', 'tp'), may hold values from -6 to 6
- in_gain: float32 [2048], replicated, may hold values from 0.1 to 1.9
- query_down: bfloat16 [2048, 512], replicated, may hold values from -0.125 to 0.125
- latent_down: bfloat16 [2048, 256], replicated, may hold values from -0.125 to 0.125
- rope_down: bfloat16 [2048, 32], replicated, may hold values from -0.125 to 0.125
- query_gain: float32 [512], replicated, may hold values from 0.5 to 12
- latent_gain: float32 [256], replicated, may hold values from 0.5 to 12
- query_nope: bfloat16 [512, 1024], P(None, 'tp'), may hold values from -0.25 to 0.25
- query_rope: bfloat16 [512, 512], P(None, 'tp'), may hold values from -0.25 to 0.25
- key_up: bfloat16 [256, 1024], P(None, 'tp'), may hold values from -0.375 to 0.375
- value_up: bfloat16 [256, 1024], P(None, 'tp'), may hold values from -0.375 to 0.375
- conv_value: bfloat16 [2048, 2048], P(None, 'tp'), may hold values from -0.125 to 0.125
- conv_gate: bfloat16 [2048, 2048], P(None, 'tp'), may hold values from -0.125 to 0.125
- conv_taps: float32 [31, 2048], P(None, 'tp'), may hold values from -1 to 1
- conv_bias: float32 [2048], P('tp'), may hold values from 0.05 to 2.25
- channel_gain: float32 [2048], P('tp'), may hold values from 0.1 to 1.9
- out_attend: bfloat16 [1024, 2048], P('tp'), may hold values from -0.109375 to 0.109375
- out_conv: bfloat16 [2048, 2048], P('tp'), may hold values from -0.109375 to 0.109375
Outputs:
- mixed: bfloat16 [2048, 2048], P('sp', 'tp')
All inputs are finite; a program needn't handle non-finite values.
Results may differ from a plain program's by a relative error of at most 0.013.
The roundings to bfloat16 on the way count: a program that leaves them out, or rounds other values in their place, can miss the bound.
Values may be sent and summed in bfloat16 or wider, within the bound.
A program may use at most 128 MiB of HBM per device.

v0:
```python
import math

import jax
import jax.numpy as jnp
from jax import lax
from jax.sharding import PartitionSpec as P

eps_norm = 1e-06
eps_layer = 1e-05
theta = 10000.0


def padded_2(cells, sides, width):
    for axis, dim in sides:
        count = lax.axis_size(axis)
        ends = count - 1
        head = lax.slice_in_dim(cells, 0, width, axis=dim)
        tail = lax.slice_in_dim(cells, cells.shape[dim] - width, cells.shape[dim], axis=dim)
        cells = jnp.concatenate(
            [
                lax.ppermute(tail, axis, [(i, (i + 1) % count) for i in range(ends)]),
                cells,
                lax.ppermute(head, axis, [((i + 1) % count, i) for i in range(ends)]),
            ],
            axis=dim,
        )
    return cells


def rms_scale(values, gain):
    return values * lax.rsqrt(jnp.mean(values * values, axis=-1, keepdims=True) + eps_norm) * gain


def rotate(values, positions):
    half = values.shape[-1] // 2
    freqs = theta ** (-jnp.arange(half).astype(jnp.float32) / half)
    angles = positions[..., None] * freqs
    cosine = jnp.cos(angles)
    sine = jnp.sin(angles)
    first = values[..., :half]
    second = values[..., half:]
    return jnp.concatenate(
        [first * cosine - second * sine, second * cosine + first * sine], axis=-1
    )


def attend_block(state, q_heads, r_heads, k_nope, values, rope_key):
    highest, total, weighted = state
    heads = q_heads.shape[1]
    key_heads = k_nope.reshape(k_nope.shape[0], heads, -1)
    value_heads = values.reshape(values.shape[0], heads, -1)
    score_scale = (q_heads.shape[2] + r_heads.shape[2]) ** (-0.5)
    scores = (
        jnp.einsum("qhd,khd->hqk", q_heads, key_heads, preferred_element_type=jnp.float32)
        + jnp.einsum("qhd,kd->hqk", r_heads, rope_key, preferred_element_type=jnp.float32)
    ) * score_scale
    new_high = jnp.maximum(highest, jnp.max(scores, axis=-1))
    factor = jnp.exp(highest - new_high)
    weight = jnp.exp(scores - new_high[..., None])
    total = total * factor + jnp.sum(weight, axis=-1)
    weighted = weighted * factor[..., None] + jnp.einsum(
        "hqk,khd->hqd", weight.astype(jnp.bfloat16), value_heads, preferred_element_type=jnp.float32
    )
    return (new_high, total, weighted)


def over_blocks(state, arrays, step):
    count = arrays[0].shape[0]
    size = math.gcd(count, 1024)
    shaped = tuple((item.reshape((count // size, size) + item.shape[1:]) for item in arrays))

    def one_block(carry, block):
        return (step(carry, block), None)

    state, unused = lax.scan(one_block, state, shaped)
    return state


def per_device(
    tokens,
    in_gain,
    query_down,
    latent_down,
    rope_down,
    query_gain,
    latent_gain,
    query_nope,
    query_rope,
    key_up,
    value_up,
    conv_value,
    conv_gate,
    conv_taps,
    conv_bias,
    channel_gain,
    out_attend,
    out_conv,
):
    row_count = tokens.shape[0]
    width = in_gain.shape[0]
    local_ch = conv_value.shape[1]
    positions = (lax.axis_index("sp") * row_count + jnp.arange(row_count)).astype(jnp.float32)
    piece_f = lax.all_gather(tokens, "tp", axis=1, tiled=True).astype(jnp.float32)
    scaled = (piece_f * in_gain).astype(jnp.bfloat16)

    def add_rows(weight):
        return jnp.dot(scaled, weight, preferred_element_type=jnp.float32)

    square_sum = jnp.sum(piece_f * piece_f, axis=1)
    q_pre = add_rows(query_down)
    kv_pre = add_rows(latent_down)
    rope_pre = add_rows(rope_down)
    value_pre = add_rows(conv_value)
    gate_pre = add_rows(conv_gate)
    row_scale = lax.rsqrt(square_sum / width + eps_norm)[:, None]
    q_latent = rms_scale(row_scale * q_pre, query_gain).astype(jnp.bfloat16)
    kv_latent = rms_scale(row_scale * kv_pre, latent_gain).astype(jnp.bfloat16)
    rope_key = rotate(row_scale * rope_pre, positions).astype(jnp.bfloat16)
    rope_size = rope_down.shape[1]
    heads = query_rope.shape[1] // rope_size
    q_heads = (
        jnp.dot(q_latent, query_nope, preferred_element_type=jnp.float32)
        .astype(jnp.bfloat16)
        .reshape(row_count, heads, -1)
    )
    q_turn = jnp.dot(q_latent, query_rope, preferred_element_type=jnp.float32).reshape(
        row_count, heads, rope_size
    )
    r_heads = rotate(q_turn, positions[:, None]).astype(jnp.bfloat16)
    value_size = value_up.shape[1] // heads
    start_state = (
        jnp.full((heads, row_count), -jnp.inf, jnp.float32),
        jnp.zeros((heads, row_count), jnp.float32),
        jnp.zeros((heads, row_count, value_size), jnp.float32),
    )

    def latent_step(state, block):
        k_nope = jnp.dot(block[0], key_up, preferred_element_type=jnp.float32).astype(jnp.bfloat16)
        values = jnp.dot(block[0], value_up, preferred_element_type=jnp.float32).astype(
            jnp.bfloat16
        )
        return attend_block(state, q_heads, r_heads, k_nope, values, block[1])

    highest, total, weighted = over_blocks(
        start_state,
        (
            lax.all_gather(kv_latent, "sp", axis=0, tiled=True),
            lax.all_gather(rope_key, "sp", axis=0, tiled=True),
        ),
        latent_step,
    )
    attended = jnp.transpose((weighted / total[..., None]).astype(jnp.bfloat16), (1, 0, 2)).reshape(
        row_count, heads * value_size
    )
    glu = (row_scale * value_pre * jax.nn.sigmoid(row_scale * gate_pre)).astype(jnp.bfloat16)
    taps = conv_taps.shape[0]
    padded = padded_2(glu, (("sp", 0),), taps // 2).astype(jnp.float32)
    conv = jnp.zeros((row_count, local_ch), jnp.float32) + conv_bias
    for tap in range(taps):
        conv = conv + conv_taps[tap] * padded[tap : tap + row_count]
    channels = local_ch * lax.axis_size("tp")
    first_sum, second_sum = lax.psum((jnp.sum(conv, axis=-1), jnp.sum(conv * conv, axis=-1)), "tp")
    mean = first_sum[:, None] / channels
    spread = second_sum[:, None] / channels - mean * mean
    centred = conv - mean
    activated = jax.nn.silu(centred * lax.rsqrt(spread + eps_layer) * channel_gain).astype(
        jnp.bfloat16
    )
    contract = (((0,), (1,)), ((), ()))
    summed = lax.psum_scatter(
        (
            lax.dot_general(out_attend, attended, contract, preferred_element_type=jnp.float32)
            + lax.dot_general(out_conv, activated, contract, preferred_element_type=jnp.float32)
        ).astype(jnp.bfloat16),
        "tp",
        scatter_dimension=0,
        tiled=True,
    ).astype(jnp.float32)
    return jnp.transpose(summed).astype(jnp.bfloat16)


def solution(mesh):
    in_specs = (
        P("sp", "tp"),
        P(),
        P(),
        P(),
        P(),
        P(),
        P(),
        P(None, "tp"),
        P(None, "tp"),
        P(None, "tp"),
        P(None, "tp"),
        P(None, "tp"),
        P(None, "tp"),
        P(None, "tp"),
        P("tp"),
        P("tp"),
        P("tp", None),
        P("tp", None),
    )
    out_specs = P("sp", "tp")
    return jax.shard_map(
        per_device, mesh=mesh, in_specs=in_specs, out_specs=out_specs, check_vma=False
    )
```

profile of v0, /device:TPU:0, one launch (start us, length us, event | category | flops | bytes accessed | tf_op | source)
XLA Modules:
  0.0 147.2 jit_solution(18445132968032190985)
XLA Ops:
  8.5 1.6 %fusion.76 = (f32[1,512]{1,0:T(1,128)}, f32[1,512]{1,0:T(1,128)}, f32[1,512]{1,0:T(1,128)}, f32[1,512]{1,0:T(1,128)}, f32[1,512]{1,0:T(1,128)}, /*index=5*/f32[1...) fusion(f32[31,512]{1,0:T(8,128)} %param.33), kind=kLoop, calls=%fused_computation.139 | loop fusion | bytes 49152 | tf_op jit(solution)/shard_map/slice | solution.py:160
  10.1 1.8 %fusion.75 = (f32[1,512]{1,0:T(1,128)}, f32[1,512]{1,0:T(1,128)}, f32[1,512]{1,0:T(1,128)}, f32[1,512]{1,0:T(1,128)}, f32[1,512]{1,0:T(1,128)}, /*index=5*/f32[1...) fusion(f32[31,512]{1,0:T(8,128)} %param.33), kind=kLoop, calls=%fused_computation.138 | loop fusion | bytes 77824 | tf_op jit(solution)/shard_map/slice | solution.py:160
  12.0 16.4 %all-gather.3.cloned.1.call-done = bf16[256,2048]{1,0:T(8,128)(2,1)} async-done(((bf16[256,512]{1,0:T(8,128)(2,1)}), bf16[256,2048]{1,0:T(8,128)(2,1)}) %all-gather.3.cloned.1.call-update) | async-done | bytes 1048592 | tf_op jit(solution)/shard_map/all_gather | solution.py:103
  28.3 1.5 %fusion.21 = f32[256]{0:T(256)S(1)} fusion(bf16[256,2048]{1,0:T(8,128)(2,1)} %all-gather.3.cloned.1.call-done), kind=kLoop, calls=%fused_computation.29 | loop fusion | flops 1572608 | bytes 1049600 | tf_op jit(solution)/shard_map/reduce_sum | solution.py:109
  29.9 2.9 %fusion.26 = f32[256,512]{1,0:T(8,128)S(1)} fusion(bf16[2048,512]{1,0:T(8,128)(2,1)} %param.32, bf16[256,2048]{1,0:T(8,128)(2,1)} %all-gather.3.cloned.1.call-done, f32[2048]{0:T(1024)} %param.21, f32[256]{0:T(256)S(1)} %add_rsqrt_fusion.3), kind=kOutput, calls=%fused_computation.35 | convolution fusion | flops 538968064 | bytes 3679232 | tf_op jit(solution)/shard_map/dot_general | solution.py:107
  34.2 4.0 %collective-permute-start = (bf16[15,512]{1,0:T(8,128)(2,1)}, bf16[15,512]{1,0:T(8,128)(2,1)}, u32[]{:S(2)}, u32[]{:S(2)}) collective-permute-start(bf16[15,512]{1,0:T(8,128)(2,1)} %get-tuple-element.132), channel_id=1, source_target_pairs={{0,4},{4,8},{8,12},{12,16},{16,20},{20,24},{24,28},{1,5},{5,9},{9,... | collective-permute-start | bytes 46088 | tf_op jit(solution)/shard_map/ppermute | solution.py:21
  38.1 1.4 collective-permute-start.1
  41.9 1.7 %convolution_multiply_fusion.4 = f32[256,32]{0,1:T(8,128)S(1)} fusion(bf16[2048,32]{0,1:T(8,128)(2,1)} %param.24, bf16[256,2048]{1,0:T(8,128)(2,1)} %all-gather.3.cloned.1.call-done, f32[2048]{0:T(1024)} %param.21, f32[256]{0:T(256)} %copy-done.41), kind=kOutput, calls=%fused_computation.42 | convolution fusion | flops 35135488 | bytes 1221632 | tf_op jit(solution)/shard_map/dot_general | solution.py:107
  45.7 1.3 convolution_convert_fusion.2
  47.0 32.4 %all_gather.11 = bf16[2048,32]{0,1:T(8,128)(2,1)S(1)} all-gather(bf16[256,32]{0,1:T(8,128)(2,1)S(1)} %pad_maximum_fusion.1), channel_id=1, replica_groups=mesh['sp'=8,'tp'=4] {'sp'}, dimensions={0}, use_global_device_ids=true | all-gather | bytes 147456 | tf_op jit(solution)/shard_map/all_gather | solution.py:148
  81.2 3.3 %fusion.71 = (f32[256]{0:T(256)S(1)}, f32[256]{0:T(256)S(1)}, f32[256,512]{1,0:T(8,128)}) fusion(f32[286,512]{1,0:T(8,128)S(1)} %maximum_convert_fusion, f32[512]{0:T(512)S(1)} %bitcast.119, f32[512]{0:T(512)S(1)} %bitcast.120, f32[512]{0:T(512)S(1)} %bitcast.122, f32[512]{0:T(512)S(1)} %bitcast.123, f32[512]{0:T(512)S(1)} %bitcast.124, ...), kind=kLoop, calls=%fused_computation.135 | loop fusion | flops 8519168 | bytes 16844800 | tf_op jit(solution)/shard_map/reduce_sum | solution.py:162
  84.5 5.6 %all-reduce = (f32[256]{0:T(256)S(1)}, f32[256]{0:T(256)S(1)}) all-reduce(f32[256]{0:T(256)S(1)} %get-tuple-element.104, f32[256]{0:T(256)S(1)} %get-tuple-element.103), channel_id=1, replica_groups=mesh['sp'=8,'tp'=4] {'tp'}, use_global_device_ids=true, to_apply=%region_10.11 | all-reduce | flops 512 | bytes 4096 | tf_op jit(solution)/shard_map/psum | solution.py:162
  90.7 1.5 %copy.23 = bf16[2048,256]{1,0:T(8,128)(2,1)S(1)} copy(bf16[2048,256]{0,1:T(8,128)(2,1)} %all-gather.5.cloned.1.call-done) | data formatting | bytes 2097152
  92.2 19.9 %while.15 = (s32[]{:T(128)}, f32[4,256]{1,0:T(4,128)S(1)}, f32[4,256]{1,0:T(4,128)S(1)}, f32[4,256,64]{1,2,0:T(8,128)S(1)}, bf16[2,1024,256]{2,1,0:T(8,128)(2,1)...) while((s32[]{:T(128)}, f32[4,256]{1,0:T(4,128)S(1)}, ...), condition=%wide.region_6.7_spmd.clone, body=%wide.region_3.6_spmd.clone.sunk | while | flops 612045824 | bytes 42795232 | solution.py:75
  92.2 1.2 convolution_convert_fusion.5
  94.4 2.7 %fusion.119 = (f32[4,256]{1,0:T(4,128)S(1)}, f32[4,256,1024]{1,2,0:T(8,128)}) fusion(bf16[256,4,32]{0,2,1:T(8,128)(2,1)S(1)} %copy-done.2, bf16[2,1024,32]{1,2,0:T(8,128)(2,1)S(1)} %copy-done.3, s32[]{:T(128)} %get-tuple-element.260, f32[4,1024,256]{2,1,0:T(8,128)S(1)} %fusion.118), kind=kOutput, calls=%fused_computation.136.clone.1 | convolution fusion | flops 70253568 | bytes 8523780 | tf_op jit(solution)/shard_map/while/body/eval_jaxpr/qhd,kd->hqk/dot_general | solution.py:55
  97.1 2.9 %fusion.120 = f32[4,256]{1,0:T(4,128)S(1)} fusion(f32[4,256,1024]{1,2,0:T(8,128)} %get-tuple-element.245, f32[4,256]{1,0:T(4,128)S(1)} %select_maximum_fusion.2), kind=kLoop, calls=%fused_computation.4.clone.1 | loop fusion | flops 2096128 | bytes 4202496 | tf_op jit(solution)/shard_map/while/body/eval_jaxpr/reduce_sum | solution.py:60
  100.0 1.3 convolution_convert_fusion.6
  104.3 2.7 %fusion.119 = (f32[4,256]{1,0:T(4,128)S(1)}, f32[4,256,1024]{1,2,0:T(8,128)}) fusion(bf16[256,4,32]{0,2,1:T(8,128)(2,1)S(1)} %copy-done.2, bf16[2,1024,32]{1,2,0:T(8,128)(2,1)S(1)} %copy-done.3, s32[]{:T(128)} %get-tuple-element.260, f32[4,1024,256]{2,1,0:T(8,128)S(1)} %fusion.118), kind=kOutput, calls=%fused_computation.136.clone.1 | convolution fusion | flops 70253568 | bytes 8523780 | tf_op jit(solution)/shard_map/while/body/eval_jaxpr/qhd,kd->hqk/dot_general | solution.py:55
  107.1 2.9 %fusion.120 = f32[4,256]{1,0:T(4,128)S(1)} fusion(f32[4,256,1024]{1,2,0:T(8,128)} %get-tuple-element.245, f32[4,256]{1,0:T(4,128)S(1)} %select_maximum_fusion.2), kind=kLoop, calls=%fused_computation.4.clone.1 | loop fusion | flops 2096128 | bytes 4202496 | tf_op jit(solution)/shard_map/while/body/eval_jaxpr/reduce_sum | solution.py:60
  110.0 1.2 convolution_convert_fusion.6
  112.2 1.7 %fusion.78 = f32[256,2048]{1,0:T(8,128)S(1)} fusion(bf16[256,256]{0,1:T(8,128)(2,1)S(1)} %bitcast.106, bf16[256,2048]{1,0:T(8,128)(2,1)} %param.36), kind=kOutput, calls=%fused_computation.141 | convolution fusion | flops 268435456 | bytes 3276800 | tf_op jit(solution)/shard_map/dot_general | solution.py:172
  113.9 1.9 %fusion.20 = bf16[2048,256]{0,1:T(8,128)(2,1)} fusion(f32[256,2048]{1,0:T(8,128)S(1)} %fusion.78, bf16[512,2048]{1,0:T(8,128)(2,1)S(1)} %copy-done, f32[256,512]{1,0:T(8,128)S(1)} %copy-done.5, f32[512]{0:T(512)S(1)} %copy-done.47, f32[256]{0:T(256)S(1)} %copy-done.42, f32[256]{0:T(256)S(1)} %get-tuple-element.173), kind=kOutput, calls=%fused_computation.28 | convolution fusion | flops 538968064 | bytes 5771264 | tf_op jit(solution)/shard_map/dot_general | solution.py:173
  115.8 24.9 %reduce-scatter.2.cloned.1.call-done = bf16[512,256]{0,1:T(8,128)(2,1)} async-done(((bf16[2048,256]{0,1:T(8,128)(2,1)}), bf16[512,256]{0,1:T(8,128)(2,1)}) %reduce-scatter.2.cloned.1.call-update) | async-done | bytes 262160 | tf_op jit(solution)/shard_map/reduce_scatter | solution.py:170
  (144 shorter events, 14.4 us)
Async XLA Ops:
  6.5 107.4 %copy-start = (bf16[512,2048]{1,0:T(8,128)(2,1)S(1)}, bf16[512,2048]{1,0:T(8,128)(2,1)}, u32[]{:S(2)}) copy-start(bf16[512,2048]{1,0:T(8,128)(2,1)} %param.37) | copy-start | bytes 6291460
  6.5 21.8 %all-gather.3.cloned.1.call-start = ((), (), s32[]{:S(2)}) async-start(), calls=%async_computation.1 | async-start | bytes 1310720 | tf_op jit(solution)/shard_map/all_gather | solution.py:103
  7.3 83.4 %all-gather.5.cloned.1.call-start = ((), (), s32[]{:S(2)}) async-start(), calls=%async_computation.2 | async-start | bytes 1179648 | tf_op jit(solution)/shard_map/all_gather | solution.py:147
  34.2 45.9 %collective-permute-start = (bf16[15,512]{1,0:T(8,128)(2,1)}, bf16[15,512]{1,0:T(8,128)(2,1)}, u32[]{:S(2)}, u32[]{:S(2)}) collective-permute-start(bf16[15,512]{1,0:T(8,128)(2,1)} %get-tuple-element.132), channel_id=1, source_target_pairs={{0,4},{4,8},{8,12},{12,16},{16,20},{20,24},{24,28},{1,5},{5,9},{9,... | collective-permute-start | bytes 46088 | tf_op jit(solution)/shard_map/ppermute | solution.py:21
  38.1 41.9 %collective-permute-start.1 = (bf16[15,512]{1,0:T(8,128)(2,1)}, bf16[15,512]{1,0:T(8,128)(2,1)}, u32[]{:S(2)}, u32[]{:S(2)}) collective-permute-start(bf16[15,512]{1,0:T(8,128)(2,1)} %get-tuple-element.133), channel_id=1, source_target_pairs={{4,0},{8,4},{12,8},{16,12},{20,16},{24,20},{28,24},{5,1},{9,5},{13... | collective-permute-start | bytes 46088 | tf_op jit(solution)/shard_map/ppermute | solution.py:23
  41.8 98.9 %reduce-scatter.2.cloned.1.call-start = ((), (), s32[]{:S(2)}) async-start(), calls=%async_computation.3 | async-start | bytes 1310720 | tf_op jit(solution)/shard_map/reduce_scatter | solution.py:170
  43.6 37.3 %copy-start.8 = (f32[1,512]{1,0:T(1,128)S(1)}, f32[1,512]{1,0:T(1,128)}, u32[]{:S(2)}) copy-start(f32[1,512]{1,0:T(1,128)} %get-tuple-element.155) | copy-start | bytes 6148
  43.6 37.3 %copy-start.9 = (f32[1,512]{1,0:T(1,128)S(1)}, f32[1,512]{1,0:T(1,128)}, u32[]{:S(2)}) copy-start(f32[1,512]{1,0:T(1,128)} %get-tuple-element.156) | copy-start | bytes 6148
  43.6 37.3 %copy-start.10 = (f32[1,512]{1,0:T(1,128)S(1)}, f32[1,512]{1,0:T(1,128)}, u32[]{:S(2)}) copy-start(f32[1,512]{1,0:T(1,128)} %get-tuple-element.157) | copy-start | bytes 6148
  43.6 37.3 %copy-start.11 = (f32[1,512]{1,0:T(1,128)S(1)}, f32[1,512]{1,0:T(1,128)}, u32[]{:S(2)}) copy-start(f32[1,512]{1,0:T(1,128)} %get-tuple-element.158) | copy-start | bytes 6148
  43.6 37.3 %copy-start.12 = (f32[1,512]{1,0:T(1,128)S(1)}, f32[1,512]{1,0:T(1,128)}, u32[]{:S(2)}) copy-start(f32[1,512]{1,0:T(1,128)} %get-tuple-element.159) | copy-start | bytes 6148
  43.6 37.3 %copy-start.13 = (f32[1,512]{1,0:T(1,128)S(1)}, f32[1,512]{1,0:T(1,128)}, u32[]{:S(2)}) copy-start(f32[1,512]{1,0:T(1,128)} %get-tuple-element.160) | copy-start | bytes 6148
  43.6 37.3 %copy-start.14 = (f32[1,512]{1,0:T(1,128)S(1)}, f32[1,512]{1,0:T(1,128)}, u32[]{:S(2)}) copy-start(f32[1,512]{1,0:T(1,128)} %get-tuple-element.161) | copy-start | bytes 6148
  43.6 37.3 %copy-start.15 = (f32[1,512]{1,0:T(1,128)S(1)}, f32[1,512]{1,0:T(1,128)}, u32[]{:S(2)}) copy-start(f32[1,512]{1,0:T(1,128)} %get-tuple-element.162) | copy-start | bytes 6148
  43.6 37.3 %copy-start.16 = (f32[1,512]{1,0:T(1,128)S(1)}, f32[1,512]{1,0:T(1,128)}, u32[]{:S(2)}) copy-start(f32[1,512]{1,0:T(1,128)} %get-tuple-element.163) | copy-start | bytes 6148
  43.6 37.3 %copy-start.17 = (f32[1,512]{1,0:T(1,128)S(1)}, f32[1,512]{1,0:T(1,128)}, u32[]{:S(2)}) copy-start(f32[1,512]{1,0:T(1,128)} %get-tuple-element.164) | copy-start | bytes 6148
  43.7 37.3 %copy-start.18 = (f32[1,512]{1,0:T(1,128)S(1)}, f32[1,512]{1,0:T(1,128)}, u32[]{:S(2)}) copy-start(f32[1,512]{1,0:T(1,128)} %get-tuple-element.165) | copy-start | bytes 6148
  43.7 37.3 %copy-start.19 = (f32[1,512]{1,0:T(1,128)S(1)}, f32[1,512]{1,0:T(1,128)}, u32[]{:S(2)}) copy-start(f32[1,512]{1,0:T(1,128)} %get-tuple-element.166) | copy-start | bytes 6148
  43.7 37.3 %copy-start.20 = (f32[1,512]{1,0:T(1,128)S(1)}, f32[1,512]{1,0:T(1,128)}, u32[]{:S(2)}) copy-start(f32[1,512]{1,0:T(1,128)} %get-tuple-element.136) | copy-start | bytes 6148
  43.7 37.3 %copy-start.21 = (f32[1,512]{1,0:T(1,128)S(1)}, f32[1,512]{1,0:T(1,128)}, u32[]{:S(2)}) copy-start(f32[1,512]{1,0:T(1,128)} %get-tuple-element.137) | copy-start | bytes 6148
  43.7 37.3 %copy-start.22 = (f32[1,512]{1,0:T(1,128)S(1)}, f32[1,512]{1,0:T(1,128)}, u32[]{:S(2)}) copy-start(f32[1,512]{1,0:T(1,128)} %get-tuple-element.138) | copy-start | bytes 6148
  43.7 37.3 %copy-start.23 = (f32[1,512]{1,0:T(1,128)S(1)}, f32[1,512]{1,0:T(1,128)}, u32[]{:S(2)}) copy-start(f32[1,512]{1,0:T(1,128)} %get-tuple-element.139) | copy-start | bytes 6148
  43.7 37.3 %copy-start.24 = (f32[1,512]{1,0:T(1,128)S(1)}, f32[1,512]{1,0:T(1,128)}, u32[]{:S(2)}) copy-start(f32[1,512]{1,0:T(1,128)} %get-tuple-element.140) | copy-start | bytes 6148
  43.7 37.3 %copy-start.25 = (f32[1,512]{1,0:T(1,128)S(1)}, f32[1,512]{1,0:T(1,128)}, u32[]{:S(2)}) copy-start(f32[1,512]{1,0:T(1,128)} %get-tuple-element.141) | copy-start | bytes 6148
  (32 other events, 577.4 us)
Sparse Core Ops, SparseCore 0:
  8.9 19.4 all-gather.2
  42.0 40.8 all-gather.4
  116.0 24.6 reduce-scatter.1
where the time goes:
time: 148 us; the launch traced here: 147 us
  waiting for transfers between devices  42 us (28%)
  blocking collectives  38 us (26%)
  matrix products  25.4 us (17%)
  other arithmetic  15.5 us (10%)
  between operations  13.9 us (9%)
  local copies, waits for them, and re-layouts  6.72 us (5%)
  starting transfers between devices  5.47 us (4%)
    all_gather x1, blocking collectives, per_device(): lax.all_gather(rope_key, 'sp', axis=0, tiled=True)  32.4 us
    reduce_scatter x1, waiting for transfers between devices, per_device(): lax.psum_scatter((lax.dot_general(out_attend, attended, contract, preferr...  24.9 us
    all_gather x1, waiting for transfers between devices, per_device(): lax.all_gather(tokens, 'tp', axis=1, tiled=True).astype(jnp.float32)  16.4 us
    dot_general x5, matrix products, add_rows(): return jnp.dot(scaled, weight, preferred_element_type=jnp.float32)  6.63 us
    reduce_sum x2, other arithmetic, attend_block(): total = total * factor + jnp.sum(weight, axis=-1)  5.81 us
    psum x1, blocking collectives, per_device(): lax.psum((jnp.sum(conv, axis=-1), jnp.sum(conv * conv, axis=-1)), 'tp')  5.63 us
    dot_general x2, matrix products, attend_block(): jnp.einsum('qhd,kd->hqk', r_heads, rope_key, preferred_element_type=jnp.f...  5.41 us
    ppermute x1, starting transfers between devices, padded_2(): lax.ppermute(tail, axis, [(i, (i + 1) % count) for i in range(ends)])  3.98 us
  transfers between devices with their start and end apart: 5, of which 2 were waited for; matrix products, arithmetic and copies ran while one was open for 11% of the time, Pallas kernels for 0%

commit v1 on v0

v1 whole, which is shorter than its diff:
```python
import functools

import jax
import jax.numpy as jnp
import numpy as np
from jax import lax
from jax.experimental import pallas as pl
from jax.experimental.pallas import tpu as pltpu
from jax.sharding import PartitionSpec as P

eps_norm = 1e-06
eps_layer = 1e-05
theta = 10000.0
LANES = 128
MESH = pl.DeviceIdType.MESH
bf16 = jnp.bfloat16
f32 = jnp.float32


def dot(a, b):
    return jnp.dot(a, b, preferred_element_type=f32)


def dot_t(a, b):
    return lax.dot_general(a, b, (((1,), (1,)), ((), ())), preferred_element_type=f32)


def body(
    n_sp, n_tp, rope, nope, heads, tchunks, rblocks, kchunk,
    tok, gain, wq, wl, wr, qgain, lgain, wqn, wqr, wku, wvu, wcv, wcg, taps, bias, cgain,
    woa, woc, cos_off, sin_off, cos_base, sin_base, spread_mat,
    out,
    v_tok, v_wq, v_wl, v_wr, v_wqn, v_wqr, v_wku, v_wvu, v_wcv, v_wcg, v_woa, v_woc, v_sp,
    acc_q, acc_l, acc_r, acc_v, acc_g,
    kvr, k_all, v_all, r_all, qf, glu_pad, conv_in, conv_out, stats, act, att,
    cpart, own_part, to_partner, from_partner, to_cross, from_cross,
    w_sem, tx_s, tx_r, tp_s, tp_r, tr_s, tr_r, kx_s, kx_r, ky_s, ky_r,
    h_s, h_r, st_s, st_r, pp_s, pp_r, cc_s, cc_r,
):
    sp, tp = lax.axis_index("sp"), lax.axis_index("tp")
    pairs = n_tp // 2
    pair, core = tp // 2, tp % 2
    partner = pair * 2 + (1 - core)
    rows, dl = tok.shape
    width = n_tp * dl
    kvw = wl.shape[1]
    half = rows // 2
    groups = kvw // rope
    prow = half // groups
    rw = heads * rope
    ch = wcv.shape[1]
    ntap = taps.shape[0]
    pad = glu_pad.shape[0] - rows
    pad = pad // 2

    def rcopy(src, dst, ssem, rsem, to_sp, to_tp):
        return pltpu.make_async_remote_copy(
            src_ref=src, dst_ref=dst, send_sem=ssem, recv_sem=rsem,
            device_id=(to_sp, to_tp), device_id_type=MESH)

    loads = {}
    for i, (name, src, dst) in enumerate([
        ("tok", tok, v_tok.at[tp]), ("wl", wl, v_wl), ("wr", wr, v_wr), ("wq", wq, v_wq),
        ("wcv", wcv, v_wcv), ("wcg", wcg, v_wcg), ("wqn", wqn, v_wqn), ("wqr", wqr, v_wqr),
        ("wku", wku, v_wku), ("wvu", wvu, v_wvu), ("sp", spread_mat, v_sp),
        ("woc", woc, v_woc), ("woa", woa, v_woa),
    ]):
        loads[name] = pltpu.make_async_copy(src, dst, w_sem.at[i])
        loads[name].start()

    barrier = pltpu.get_barrier_semaphore()
    for d in range(1, n_tp):
        pl.semaphore_signal(barrier, inc=1, device_id=(sp, (tp + d) % n_tp), device_id_type=MESH)
    for d in range(1, n_sp):
        pl.semaphore_signal(barrier, inc=1, device_id=((sp + d) % n_sp, tp), device_id_type=MESH)
    pl.semaphore_wait(barrier, n_tp - 1 + n_sp - 1)

    tr = rows // tchunks
    sends = []
    for j in range(1, pairs):
        for r in range(tchunks):
            part = pl.ds(r * tr, tr)
            c = rcopy(tok.at[part], v_tok.at[tp, part], tx_s.at[j, r], tx_r.at[j, r],
                      sp, ((pair + j) % pairs) * 2 + core)
            c.start()
            sends.append(c)
    to_p = rcopy(tok, v_tok.at[tp], tp_s, tp_r, sp, partner)
    to_p.start()
    sends.append(to_p)

    def shard(t):
        x = v_tok[t].astype(f32)
        g = gain[:, pl.ds(pl.multiple_of(t * dl, LANES), dl)]
        return (x * g).astype(bf16), jnp.sum(x * x, axis=1, keepdims=True)

    def wrows(ref, t):
        return ref[pl.ds(pl.multiple_of(t * dl, LANES), dl), :]

    everything = ((acc_l, v_wl), (acc_r, v_wr), (acc_q, v_wq), (acc_v, v_wcv), (acc_g, v_wcg))
    loads["tok"].wait()
    xs, sq = shard(tp)
    for name in ("wl", "wr", "wq", "wcv", "wcg"):
        loads[name].wait()
    for acc, w in everything:
        acc[...] = dot(xs, wrows(w, tp))
    to_p.wait_recv()
    xs, s = shard(partner)
    sq = sq + s
    for acc, w in everything:
        acc[...] += dot(xs, wrows(w, partner))
    for j in range(1, pairs):
        src_t = ((pair + pairs - j) % pairs) * 2 + core
        for r in range(tchunks):
            part = pl.ds(r * tr, tr)
            rcopy(tok.at[part], v_tok.at[src_t, part], tx_s.at[j, r], tx_r.at[j, r], sp, partner).wait_recv()
            c = rcopy(v_tok.at[src_t, part], v_tok.at[src_t, part], tr_s.at[j, r], tr_r.at[j, r], sp, partner)
            c.start()
            sends.append(c)
    rest = []
    for j in range(1, pairs):
        base = ((pair + pairs - j) % pairs) * 2
        xs, s = shard(base + core)
        sq = sq + s
        acc_l[...] += dot(xs, wrows(v_wl, base + core))
        acc_r[...] += dot(xs, wrows(v_wr, base + core))
        rest.append((xs, base + core))
    for j in range(1, pairs):
        base = ((pair + pairs - j) % pairs) * 2
        other = base + (1 - core)
        for r in range(tchunks):
            part = pl.ds(r * tr, tr)
            rcopy(v_tok.at[other, part], v_tok.at[other, part], tr_s.at[j, r], tr_r.at[j, r], sp, partner).wait_recv()
        xs, s = shard(other)
        sq = sq + s
        acc_l[...] += dot(xs, wrows(v_wl, other))
        acc_r[...] += dot(xs, wrows(v_wr, other))
        rest.append((xs, other))
    row_scale = lax.rsqrt(sq * (1.0 / width) + eps_norm)

    def rms(v, g):
        return v * lax.rsqrt(jnp.mean(v * v, axis=-1, keepdims=True) + eps_norm) * g

    cb, sb = cos_base[pl.ds(sp, 1), :], sin_base[pl.ds(sp, 1), :]
    co, so = cos_off[...], sin_off[...]
    cosine = cb * co - sb * so
    sine = sb * co + cb * so

    def turn(v, w):
        lane = lax.broadcasted_iota(jnp.int32, v.shape, 1)
        first = None
        for g in range(w // rope):
            m = (lane >= g * rope) & (lane < g * rope + rope // 2)
            first = m if first is None else first | m
        up = pltpu.roll(v, w - rope // 2, axis=1)
        down = pltpu.roll(v, rope // 2, axis=1)
        return v * cosine[:, :w] + jnp.where(first, -up, down) * sine[:, :w]

    kv = rms(row_scale * acc_l[...], lgain[...]).astype(bf16)
    rk = row_scale * acc_r[...]
    rk = turn(jnp.concatenate([rk] * groups, axis=1), kvw)
    lane_p = lax.broadcasted_iota(jnp.int32, (prow, kvw), 1)
    for hf in range(2):
        kvr[sp, hf, 0:half, :] = kv[hf * half:(hf + 1) * half]
        packed = jnp.zeros((prow, kvw), f32)
        for g in range(groups):
            piece = rk[hf * half + g * prow: hf * half + (g + 1) * prow]
            packed = jnp.where((lane_p >= g * rope) & (lane_p < (g + 1) * rope), piece, packed)
        kvr[sp, hf, half:half + prow, :] = packed.astype(bf16)
    for d in range(1, n_sp):
        c = rcopy(kvr.at[sp, core], kvr.at[sp, core], kx_s.at[d], kx_r.at[d], (sp + d) % n_sp, tp)
        c.start()
        sends.append(c)

    for xs, t in rest:
        acc_v[...] += dot(xs, wrows(v_wcv, t))
        acc_g[...] += dot(xs, wrows(v_wcg, t))
    glu = (row_scale * acc_v[...] * jax.nn.sigmoid(row_scale * acc_g[...])).astype(bf16)
    glu_pad[pad:pad + rows, :] = glu
    zeros_halo = jnp.zeros((pad, ch), bf16)

    def halo(up):
        if up:
            return rcopy(glu_pad.at[pl.ds(rows, pad)], glu_pad.at[pl.ds(0, pad)],
                         h_s.at[0], h_r.at[0], (sp + 1) % n_sp, tp)
        return rcopy(glu_pad.at[pl.ds(pad, pad)], glu_pad.at[pl.ds(pad + rows, pad)],
                     h_s.at[1], h_r.at[1], (sp + n_sp - 1) % n_sp, tp)

    @pl.when(sp < n_sp - 1)
    def _():
        halo(True).start()

    @pl.when(sp > 0)
    def _():
        halo(False).start()

    @pl.when(sp == 0)
    def _():
        glu_pad[0:pad, :] = zeros_halo

    @pl.when(sp == n_sp - 1)
    def _():
        glu_pad[pad + rows:pad + rows + pad, :] = zeros_halo

    for xs, t in rest:
        acc_q[...] += dot(xs, wrows(v_wq, t))
    ql = rms(row_scale * acc_q[...], qgain[...]).astype(bf16)
    for name in ("wqn", "wqr"):
        loads[name].wait()
    qn = dot(ql, v_wqn[...])
    qr = turn(dot(ql, v_wqr[...]), rw)
    per = LANES // nope
    lane_n = lax.broadcasted_iota(jnp.int32, (rows, LANES), 1)
    lane_r = lax.broadcasted_iota(jnp.int32, (rows, rw), 1)
    for h in range(heads):
        blk, off = h // per, (h % per) * nope
        qf[h, :, 0:LANES] = jnp.where(
            (lane_n >= off) & (lane_n < off + nope), qn[:, blk * LANES:(blk + 1) * LANES], 0.0).astype(bf16)
        qf[h, :, LANES:LANES + rw] = jnp.where(
            (lane_r >= h * rope) & (lane_r < (h + 1) * rope), qr, 0.0).astype(bf16)

    def relay(d, start):
        src = (sp + n_sp - d) % n_sp
        if start:
            rcopy(kvr.at[src, core], kvr.at[src, core], kx_s.at[d], kx_r.at[d], sp, partner).wait_recv()
            c = rcopy(kvr.at[src, core], kvr.at[src, core], ky_s.at[d], ky_r.at[d], sp, partner)
            c.start()
            sends.append(c)
        else:
            other = kvr.at[src, 1 - core]
            rcopy(other, other, ky_s.at[d], ky_r.at[d], sp, partner).wait_recv()

    @pl.when(sp < n_sp - 1)
    def _():
        halo(True).wait_send()
        halo(False).wait_recv()

    @pl.when(sp > 0)
    def _():
        halo(False).wait_send()
        halo(True).wait_recv()

    conv_in[...] = glu_pad[...].astype(f32)
    rb = rows // 2
    first_off = pad - ntap // 2
    s1, s2 = [], []
    for b in range(2):
        t1 = jnp.zeros((rb, LANES), f32)
        t2 = jnp.zeros((rb, LANES), f32)
        for l in range(ch // LANES):
            cols = slice(l * LANES, (l + 1) * LANES)
            x = conv_in[b * rb:b * rb + rb + 2 * pad, cols]
            n = rb + 2 * pad
            acc = jnp.zeros((rb, LANES), f32) + bias[:, cols]
            for res in range(8):
                xr = x if res == 0 else pltpu.roll(x, n - res, axis=0)
                for k in range(ntap):
                    if (k + first_off) % 8 == res:
                        o = k + first_off - res
                        acc = acc + taps[k:k + 1, cols] * xr[o:o + rb]
            conv_out[b * rb:(b + 1) * rb, cols] = acc
            t1 = t1 + acc
            t2 = t2 + acc * acc
        s1.append(jnp.sum(t1, axis=1, keepdims=True))
        s2.append(jnp.sum(t2, axis=1, keepdims=True))
    s1 = jnp.concatenate(s1, axis=0)
    s2 = jnp.concatenate(s2, axis=0)
    lane_s = lax.broadcasted_iota(jnp.int32, (rows, LANES), 1)
    stats[tp] = jnp.transpose(jnp.where(lane_s == 0, s1, jnp.where(lane_s == 1, s2, 0.0)))[0:8]
    for d in range(1, n_tp):
        c = rcopy(stats.at[tp], stats.at[tp], st_s.at[d], st_r.at[d], sp, (tp + d) % n_tp)
        c.start()
        sends.append(c)
    order = list(range(1, n_sp))
    for d in order:
        relay(d, True)

    for d in range(1, n_tp):
        src = (tp + n_tp - d) % n_tp
        rcopy(stats.at[src], stats.at[src], st_s.at[d], st_r.at[d], sp, partner).wait_recv()
    tot = stats[0]
    for t in range(1, n_tp):
        tot = tot + stats[t]
    tot = jnp.transpose(jnp.concatenate([tot, jnp.zeros((LANES - 8, rows), f32)], axis=0))
    mean = tot[:, 0:1] * (1.0 / (ch * n_tp))
    var = tot[:, 1:2] * (1.0 / (ch * n_tp)) - mean * mean
    y = (conv_out[...] - mean) * lax.rsqrt(var + eps_layer) * cgain[...]
    act[...] = (y * jax.nn.sigmoid(y)).astype(bf16)
    loads["woc"].wait()
    cpart[...] = dot(act[...], v_woc[...])

    for d in order:
        relay(d, False)

    for name in ("wku", "wvu", "sp"):
        loads[name].wait()

    def expand(s, _):
        for hf in range(2):
            lat = kvr[s, hf, 0:half, :]
            at = pl.ds(pl.multiple_of(s * rows, rows) + hf * half, half)
            k_all[at, :] = dot(lat, v_wku[...]).astype(bf16)
            v_all[at, :] = dot(lat, v_wvu[...]).astype(bf16)
            u = dot(kvr[s, hf, half:half + prow, :], v_sp[...]).astype(bf16)
            for g in range(groups):
                r_all[pl.ds(pl.multiple_of(s * rows, rows) + hf * half + g * prow, prow), :] = u[:, g * rw:(g + 1) * rw]
        return 0

    lax.fori_loop(0, n_sp, expand, 0)

    keys = n_sp * rows
    nk = keys // kchunk
    qb = rows // rblocks
    vw = v_all.shape[1]
    vdim = vw // heads
    scale2 = float((nope + rope) ** -0.5 * np.log2(np.e))
    lane_v = lax.broadcasted_iota(jnp.int32, (qb, vw), 1)

    def attend(b, hs, result):
        for h in hs:
            blk = h // per
            q = qf[h, b * qb:(b + 1) * qb, :]

            def scores(at):
                k = jnp.concatenate([k_all[at, blk * LANES:(blk + 1) * LANES], r_all[at, :]], axis=1)
                return dot_t(q, k)

            if nk == 1:
                at = slice(0, keys)
                s = scores(at)
                m = jnp.max(s, axis=1, keepdims=True)
                w = jnp.exp2((s - m) * scale2)
                total = jnp.sum(w, axis=1, keepdims=True)
                o = dot(w.astype(bf16), v_all[at, :])
            else:
                def step(i, carry):
                    m, total, o = carry
                    at = pl.ds(pl.multiple_of(i * kchunk, kchunk), kchunk)
                    s = scores(at)
                    nm = jnp.maximum(m, jnp.max(s, axis=1, keepdims=True))
                    f = jnp.exp2((m - nm) * scale2)
                    w = jnp.exp2((s - nm) * scale2)
                    return (nm, total * f + jnp.sum(w, axis=1, keepdims=True),
                            o * f + dot(w.astype(bf16), v_all[at, :]))
                m, total, o = lax.fori_loop(0, nk, step, (
                    jnp.full((qb, 1), -jnp.inf, f32), jnp.zeros((qb, 1), f32), jnp.zeros((qb, vw), f32)))
            mask = (lane_v >= h * vdim) & (lane_v < (h + 1) * vdim)
            result = jnp.where(mask, o / total, result)
        return result

    def partial(b, t, a):
        cols = pl.ds(pl.multiple_of(t * dl, LANES), dl)
        return (dot(a, v_woa[:, cols]) + cpart[b * qb:(b + 1) * qb, cols]).astype(bf16)

    def pcopy(b, j):
        return rcopy(to_partner.at[b, j], from_partner.at[b, j], pp_s.at[b, j], pp_r.at[b, j], sp, partner)

    def ccopy(b, j):
        return rcopy(to_cross.at[b, j], from_cross.at[b, j], cc_s.at[b, j], cc_r.at[b, j],
                     sp, ((pair + j) % pairs) * 2 + core)

    def project(b, a):
        for j in list(range(1, pairs)) + [0]:
            t = ((pair + j) % pairs) * 2
            to_partner[b, j] = partial(b, t + (1 - core), a)
            pcopy(b, j).start()
        for j in range(pairs):
            t = ((pair + j) % pairs) * 2
            own_part[b, j] = partial(b, t + core, a)

    def cross(b):
        for j in range(1, pairs):
            pcopy(b, j).wait_recv()
            to_cross[b, j] = (own_part[b, j].astype(f32) + from_partner[b, j].astype(f32)).astype(bf16)
            ccopy(b, j).start()

    zero = jnp.zeros((qb, vw), f32)
    loads["woa"].wait()
    for b in range(rblocks):
        a = attend(b, range(heads // 2), zero)
        if b:
            cross(b - 1)
        a = attend(b, range(heads // 2, heads), a)
        project(b, a.astype(bf16))
    cross(rblocks - 1)
    for b in range(rblocks):
        pcopy(b, 0).wait_recv()
        total = own_part[b, 0].astype(f32) + from_partner[b, 0].astype(f32)
        for j in range(1, pairs):
            ccopy(b, j).wait_recv()
            total = total + from_cross[b, j].astype(f32)
        out[b * qb:(b + 1) * qb, :] = total.astype(bf16)
    for b in range(rblocks):
        for j in range(pairs):
            pcopy(b, j).wait_send()
        for j in range(1, pairs):
            ccopy(b, j).wait_send()
    for c in sends:
        c.wait_send()


def per_device(n_sp, n_tp, *args):
    (tokens, in_gain, query_down, latent_down, rope_down, query_gain, latent_gain, query_nope,
     query_rope, key_up, value_up, conv_value, conv_gate, conv_taps, conv_bias, channel_gain,
     out_attend, out_conv) = args
    rows, dl = tokens.shape
    rope = rope_down.shape[1]
    heads = query_rope.shape[1] // rope
    nope = query_nope.shape[1] // heads
    kvw, qw = latent_down.shape[1], query_down.shape[1]
    ch = conv_value.shape[1]
    groups, half = kvw // rope, rows // 2
    prow = half // groups
    rw = heads * rope
    pairs = n_tp // 2
    tchunks, rblocks = 4, 2
    keys = n_sp * rows
    kchunk = min(keys, 2048)
    qb = rows // rblocks
    pad = -(-(conv_taps.shape[0] // 2) // 16) * 16
    freqs = np.float64(theta) ** (-np.arange(rope // 2) / (rope // 2))
    freqs = np.tile(freqs, 2 * groups)[None, :]
    off = np.arange(rows)[:, None] * freqs
    base = (np.arange(n_sp) * rows)[:, None] * freqs
    tables = [np.cos(off), np.sin(off), np.cos(base), np.sin(base)]
    tables = [jnp.asarray(t.astype(np.float32)) for t in tables]
    l = np.arange(kvw)[:, None]
    m = np.arange(groups * rw)[None, :]
    spread_mat = jnp.asarray(((l // rope == m // rw) & (l % rope == m % rope)).astype(np.float32), bf16)
    row = lambda v: v.reshape(1, -1)
    ins = (tokens, row(in_gain), query_down, latent_down, rope_down, row(query_gain), row(latent_gain),
           query_nope, query_rope, key_up, value_up, conv_value, conv_gate, conv_taps, row(conv_bias),
           row(channel_gain), out_attend, out_conv, *tables, spread_mat)
    A, V = pl.BlockSpec(memory_space=pl.ANY), pl.BlockSpec(memory_space=pltpu.VMEM)
    specs = [A, V, A, A, A, V, V, A, A, A, A, A, A, V, V, V, A, A, V, V, V, V, A]
    vm = lambda a: pltpu.VMEM(a.shape, a.dtype)
    D = lambda *s: pltpu.SemaphoreType.DMA(s)
    scratch = [
        pltpu.VMEM((n_tp, rows, dl), bf16), vm(query_down), vm(latent_down), vm(rope_down),
        vm(query_nope), vm(query_rope), vm(key_up), vm(value_up), vm(conv_value), vm(conv_gate),
        vm(out_attend), vm(out_conv), vm(spread_mat),
        pltpu.VMEM((rows, qw), f32), pltpu.VMEM((rows, kvw), f32), pltpu.VMEM((rows, rope), f32),
        pltpu.VMEM((rows, ch), f32), pltpu.VMEM((rows, ch), f32),
        pltpu.VMEM((n_sp, 2, half + prow, kvw), bf16),
        pltpu.VMEM((keys, key_up.shape[1]), bf16), pltpu.VMEM((keys, value_up.shape[1]), bf16),
        pltpu.VMEM((keys, rw), bf16), pltpu.VMEM((heads, rows, LANES + rw), bf16),
        pltpu.VMEM((rows + 2 * pad, ch), bf16), pltpu.VMEM((rows + 2 * pad, ch), f32),
        pltpu.VMEM((rows, ch), f32), pltpu.VMEM((n_tp, 8, rows), f32), pltpu.VMEM((rows, ch), bf16),
        pltpu.VMEM((8, LANES), f32),
        pltpu.VMEM((rows, n_tp * dl), f32),
        pltpu.VMEM((rblocks, pairs, qb, dl), bf16), pltpu.VMEM((rblocks, pairs, qb, dl), bf16),
        pltpu.VMEM((rblocks, pairs, qb, dl), bf16), pltpu.VMEM((rblocks, pairs, qb, dl), bf16),
        pltpu.VMEM((rblocks, pairs, qb, dl), bf16),
        D(13), D(pairs, tchunks), D(pairs, tchunks), pltpu.SemaphoreType.DMA, pltpu.SemaphoreType.DMA,
        D(pairs, tchunks), D(pairs, tchunks), D(n_sp), D(n_sp), D(n_sp), D(n_sp),
        D(2), D(2), D(n_tp), D(n_tp), D(rblocks, pairs), D(rblocks, pairs),
        D(rblocks, pairs), D(rblocks, pairs),
    ]
    return pl.pallas_call(
        functools.partial(body, n_sp, n_tp, rope, nope, heads, tchunks, rblocks, kchunk),
        out_shape=jax.ShapeDtypeStruct((rows, dl), bf16),
        in_specs=specs,
        out_specs=V,
        scratch_shapes=scratch,
        compiler_params=pltpu.CompilerParams(
            collective_id=0, has_side_effects=True, vmem_limit_bytes=60 * 1024 * 1024),
        name="layer",
    )(*ins)


def solution(mesh):
    in_specs = (
        P("sp", "tp"), P(), P(), P(), P(), P(), P(), P(None, "tp"), P(None, "tp"), P(None, "tp"),
        P(None, "tp"), P(None, "tp"), P(None, "tp"), P(None, "tp"), P("tp"), P("tp"),
        P("tp", None), P("tp", None),
    )
    return jax.shard_map(
        functools.partial(per_device, mesh.shape["sp"], mesh.shape["tp"]),
        mesh=mesh, in_specs=in_specs, out_specs=P("sp", "tp"), check_vma=False)
```

time: 148 us -> 55.8 us (0.38)
  the two profiles are of different devices: /device:TPU:0 before, /device:TPU:12 now
where the time goes in v1:
time: 55.8 us; the launch traced here: 55.6 us
  Pallas kernels  52 us (93%)
  local copies, waits for them, and re-layouts  3.57 us (6%)
    pallas_call x1, Pallas kernels, per_device(): pl.pallas_call(functools.partial(body, n_sp, n_tp, rope, nope, heads, tch...  52 us
    unnamed x2, local copies, waits for them, and re-layouts  3.57 us

profile of v1, /device:TPU:12, one launch (start us, length us, event | category | flops | bytes accessed | tf_op | source)
XLA Modules:
  0.0 55.6 jit_solution(6118935293135594944)
XLA Ops:
  0.0 1.9 %copy.24.wr = bf16[2048,32]{1,0:T(8,128)(2,1)} copy(bf16[2048,32]{0,1:T(8,128)(2,1)} %param.27) | data formatting | bytes 262144 | tf_op args[4]
  1.9 52.0 %layer.1 = bf16[256,512]{1,0:T(8,128)(2,1)} custom-call(bf16[256,512]{1,0:T(8,128)(2,1)} %tok.1, f32[1,2048]{1,0:T(1,128)} %bitcast.5, bf16[2048,512]{1,0:T(8,128)(2,1)} %wq.1, bf16[2048,256]{1,0:T(8,128)(2,1)} %wl.1, bf16[2048,32]{1,0:T(8,128)(2,1)} %copy.24.wr, f32[1,512]{1,0:T(1,128)} %bitcast.6, f32[1,256]{1,0:T(1,128)} %bitcast.9, ...), custom_call_target="tpu_custom_call" | custom-call | tf_op jit(solution)/shard_map/layer/pallas_call | solution.py:458
  53.9 1.7 %copy.26 = bf16[256,512]{1,0:T(8,128)(2,1)} copy(bf16[256,512]{1,0:T(8,128)(2,1)} %layer.1) | data formatting | bytes 524288

commit v2 on v1

--- a/solution.py
+++ b/solution.py
@@ -27,15 +27,16 @@
 
 def body(
     n_sp, n_tp, rope, nope, heads, tchunks, rblocks, kchunk,
-    tok, gain, wq, wl, wr, qgain, lgain, wqn, wqr, wku, wvu, wcv, wcg, taps, bias, cgain,
-    woa, woc, cos_off, sin_off, cos_base, sin_base, spread_mat,
+    tok, gain_in, wq, wl, wr, qgain_in, lgain_in, wqn, wqr, wku, wvu, wcv, wcg, taps_in, bias_in,
+    cgain_in, woa, woc, cos_off_in, sin_off_in, cos_base_in, sin_base_in, spread_mat,
     out,
     v_tok, v_wq, v_wl, v_wr, v_wqn, v_wqr, v_wku, v_wvu, v_wcv, v_wcg, v_woa, v_woc, v_sp,
+    gain, qgain, lgain, taps, bias, cgain, cos_off, sin_off, cos_base, sin_base,
     acc_q, acc_l, acc_r, acc_v, acc_g,
-    kvr, k_all, v_all, r_all, qf, glu_pad, conv_in, conv_out, stats, act, att,
-    cpart, own_part, to_partner, from_partner, to_cross, from_cross,
-    w_sem, tx_s, tx_r, tp_s, tp_r, tr_s, tr_r, kx_s, kx_r, ky_s, ky_r,
-    h_s, h_r, st_s, st_r, pp_s, pp_r, cc_s, cc_r,
+    kvr, k_all, v_all, r_all, qf, glu_pad, conv_in, conv_out, stats, act,
+    cpart, own_part, to_partner, from_partner, to_cross, from_cross, result,
+    w_sem, tx_s, tx_r, tp_s, tp_r, tr_s, tr_r, ku_s, kd_s, kz_s, kx_r, ky_s, ky_r,
+    h_s, h_r, st_s, st_r, pp_s, pp_r, cc_s, cc_r, out_s,
 ):
     sp, tp = lax.axis_index("sp"), lax.axis_index("tp")
     pairs = n_tp // 2
@@ -60,9 +61,12 @@
 
     loads = {}
     for i, (name, src, dst) in enumerate([
-        ("tok", tok, v_tok.at[tp]), ("wl", wl, v_wl), ("wr", wr, v_wr), ("wq", wq, v_wq),
+        ("tok", tok, v_tok.at[tp]), ("gain", gain_in, gain), ("wl", wl, v_wl), ("wr", wr, v_wr), ("wq", wq, v_wq),
         ("wcv", wcv, v_wcv), ("wcg", wcg, v_wcg), ("wqn", wqn, v_wqn), ("wqr", wqr, v_wqr),
-        ("wku", wku, v_wku), ("wvu", wvu, v_wvu), ("sp", spread_mat, v_sp),
+        ("wku", wku, v_wku), ("wvu", wvu, v_wvu), ("lgain", lgain_in, lgain), ("qgain", qgain_in, qgain),
+        ("co", cos_off_in, cos_off), ("so", sin_off_in, sin_off), ("cb", cos_base_in, cos_base),
+        ("sb", sin_base_in, sin_base), ("taps", taps_in, taps), ("bias", bias_in, bias),
+        ("cgain", cgain_in, cgain), ("sp", spread_mat, v_sp),
         ("woc", woc, v_woc), ("woa", woa, v_woa),
     ]):
         loads[name] = pltpu.make_async_copy(src, dst, w_sem.at[i])
@@ -71,9 +75,13 @@
     barrier = pltpu.get_barrier_semaphore()
     for d in range(1, n_tp):
         pl.semaphore_signal(barrier, inc=1, device_id=(sp, (tp + d) % n_tp), device_id_type=MESH)
-    for d in range(1, n_sp):
-        pl.semaphore_signal(barrier, inc=1, device_id=((sp + d) % n_sp, tp), device_id_type=MESH)
-    pl.semaphore_wait(barrier, n_tp - 1 + n_sp - 1)
+    for d in (1, 2):
+        for ok, to in ((sp + d < n_sp, (sp + d) % n_sp), (sp >= d, (sp + n_sp - d) % n_sp)):
+            @pl.when(ok)
+            def _():
+                pl.semaphore_signal(barrier, inc=1, device_id=(to, tp), device_id_type=MESH)
+    near = jnp.minimum(n_sp - 1 - sp, 2) + jnp.minimum(sp, 2)
+    pl.semaphore_wait(barrier, n_tp - 1 + near)
 
     tr = rows // tchunks
     sends = []
@@ -96,18 +104,26 @@
     def wrows(ref, t):
         return ref[pl.ds(pl.multiple_of(t * dl, LANES), dl), :]
 
-    everything = ((acc_l, v_wl), (acc_r, v_wr), (acc_q, v_wq), (acc_v, v_wcv), (acc_g, v_wcg))
+    def rope_rows(xs, t):
+        return dot_t(xs, v_wr[:, pl.ds(pl.multiple_of(t * dl, LANES), dl)])
+
+    everything = ((acc_l, v_wl), (acc_q, v_wq), (acc_v, v_wcv), (acc_g, v_wcg))
     loads["tok"].wait()
+    loads["gain"].wait()
     xs, sq = shard(tp)
     for name in ("wl", "wr", "wq", "wcv", "wcg"):
         loads[name].wait()
     for acc, w in everything:
         acc[...] = dot(xs, wrows(w, tp))
+    acc_r[...] = rope_rows(xs, tp)
+    for name in ("lgain", "qgain", "co", "so", "cb", "sb", "taps", "bias", "cgain"):
+        loads[name].wait()
     to_p.wait_recv()
     xs, s = shard(partner)
     sq = sq + s
     for acc, w in everything:
         acc[...] += dot(xs, wrows(w, partner))
+    acc_r[...] += rope_rows(xs, partner)
     for j in range(1, pairs):
         src_t = ((pair + pairs - j) % pairs) * 2 + core
         for r in range(tchunks):
@@ -122,7 +138,7 @@
         xs, s = shard(base + core)
         sq = sq + s
         acc_l[...] += dot(xs, wrows(v_wl, base + core))
-        acc_r[...] += dot(xs, wrows(v_wr, base + core))
+        acc_r[...] += rope_rows(xs, base + core)
         rest.append((xs, base + core))
     for j in range(1, pairs):
         base = ((pair + pairs - j) % pairs) * 2
@@ -133,7 +149,7 @@
         xs, s = shard(other)
         sq = sq + s
         acc_l[...] += dot(xs, wrows(v_wl, other))
-        acc_r[...] += dot(xs, wrows(v_wr, other))
+        acc_r[...] += rope_rows(xs, other)
         rest.append((xs, other))
     row_scale = lax.rsqrt(sq * (1.0 / width) + eps_norm)
 
@@ -154,6 +170,36 @@
         up = pltpu.roll(v, w - rope // 2, axis=1)
         down = pltpu.roll(v, rope // 2, axis=1)
         return v * cosine[:, :w] + jnp.where(first, -up, down) * sine[:, :w]
+
+    for xs, t in rest:
+        acc_v[...] += dot(xs, wrows(v_wcv, t))
+        acc_g[...] += dot(xs, wrows(v_wcg, t))
+    glu = (row_scale * acc_v[...] * jax.nn.sigmoid(row_scale * acc_g[...])).astype(bf16)
+    glu_pad[pad:pad + rows, :] = glu
+    zeros_halo = jnp.zeros((pad, ch), bf16)
+
+    def halo(up):
+        if up:
+            return rcopy(glu_pad.at[pl.ds(rows, pad)], glu_pad.at[pl.ds(0, pad)],
+                         h_s.at[0], h_r.at[0], (sp + 1) % n_sp, tp)
+        return rcopy(glu_pad.at[pl.ds(pad, pad)], glu_pad.at[pl.ds(pad + rows, pad)],
+                     h_s.at[1], h_r.at[1], (sp + n_sp - 1) % n_sp, tp)
+
+    @pl.when(sp < n_sp - 1)
+    def _():
+        halo(True).start()
+
+    @pl.when(sp > 0)
+    def _():
+        halo(False).start()
+
+    @pl.when(sp == 0)
+    def _():
+        glu_pad[0:pad, :] = zeros_halo
+
+    @pl.when(sp == n_sp - 1)
+    def _():
+        glu_pad[pad + rows:pad + rows + pad, :] = zeros_halo
 
     kv = rms(row_scale * acc_l[...], lgain[...]).astype(bf16)
     rk = row_scale * acc_r[...]
@@ -166,40 +212,75 @@
             piece = rk[hf * half + g * prow: hf * half + (g + 1) * prow]
             packed = jnp.where((lane_p >= g * rope) & (lane_p < (g + 1) * rope), piece, packed)
         kvr[sp, hf, half:half + prow, :] = packed.astype(bf16)
-    for d in range(1, n_sp):
-        c = rcopy(kvr.at[sp, core], kvr.at[sp, core], kx_s.at[d], kx_r.at[d], (sp + d) % n_sp, tp)
-        c.start()
-        sends.append(c)
-
-    for xs, t in rest:
-        acc_v[...] += dot(xs, wrows(v_wcv, t))
-        acc_g[...] += dot(xs, wrows(v_wcg, t))
-    glu = (row_scale * acc_v[...] * jax.nn.sigmoid(row_scale * acc_g[...])).astype(bf16)
-    glu_pad[pad:pad + rows, :] = glu
-    zeros_halo = jnp.zeros((pad, ch), bf16)
-
-    def halo(up):
-        if up:
-            return rcopy(glu_pad.at[pl.ds(rows, pad)], glu_pad.at[pl.ds(0, pad)],
-                         h_s.at[0], h_r.at[0], (sp + 1) % n_sp, tp)
-        return rcopy(glu_pad.at[pl.ds(pad, pad)], glu_pad.at[pl.ds(pad + rows, pad)],
-                     h_s.at[1], h_r.at[1], (sp + n_sp - 1) % n_sp, tp)
-
-    @pl.when(sp < n_sp - 1)
-    def _():
-        halo(True).start()
-
-    @pl.when(sp > 0)
-    def _():
-        halo(False).start()
-
-    @pl.when(sp == 0)
-    def _():
-        glu_pad[0:pad, :] = zeros_halo
-
-    @pl.when(sp == n_sp - 1)
-    def _():
-        glu_pad[pad + rows:pad + rows + pad, :] = zeros_halo
+    line, place, side = n_sp // 2, sp // 2, sp % 2
+
+    def block(src, sems, to_sp, to_tp, recv, hf=core):
+        ref = kvr.at[src, hf]
+        return rcopy(ref, ref, sems.at[src], recv.at[src], to_sp, to_tp)
+
+    def when(cond, f):
+        @pl.when(cond)
+        def _():
+            f()
+
+    def passes(src, mode):
+        act_on = lambda c: getattr(c, mode)()
+        act_on(block(src, kz_s, place * 2 + 1 - side, tp, kx_r))
+
+    def to_partner_core(src, mode):
+        getattr(block(src, ky_s, sp, partner, ky_r), mode)()
+
+    def up(src, mode):
+        when(place < line - 1, lambda: getattr(block(src, ku_s, (sp + 2) % n_sp, tp, kx_r), mode)())
+
+    def down(src, mode):
+        when(place > 0, lambda: getattr(block(src, kd_s, (sp + n_sp - 2) % n_sp, tp, kx_r), mode)())
+
+    def arrived(src):
+        block(src, kz_s, sp, partner, kx_r).wait_recv()
+
+    def spread_step(k, mode):
+        go = mode == "start"
+        if k == 0:
+            up(sp, mode)
+            down(sp, mode)
+            passes(sp, mode)
+            return
+
+        def below():
+            src = sp - 2 * k
+            if go:
+                arrived(src)
+            up(src, mode)
+            passes(src, mode)
+            to_partner_core(src, mode)
+
+        def above():
+            src = sp + 2 * k
+            if go:
+                arrived(src)
+            down(src, mode)
+            passes(src, mode)
+            to_partner_core(src, mode)
+
+        when(place >= k, below)
+        when(place + k < line, above)
+
+    def other_side(k, mode):
+        mine = place * 2 + 1 - side
+
+        def one(src):
+            if mode == "start":
+                arrived(src)
+            to_partner_core(src, mode)
+
+        if k == 0:
+            one(mine)
+            return
+        when(place >= k, lambda: one(mine - 2 * k))
+        when(place + k < line, lambda: one(mine + 2 * k))
+
+    spread_step(0, "start")
 
     for xs, t in rest:
         acc_q[...] += dot(xs, wrows(v_wq, t))
@@ -217,17 +298,6 @@
             (lane_n >= off) & (lane_n < off + nope), qn[:, blk * LANES:(blk + 1) * LANES], 0.0).astype(bf16)
         qf[h, :, LANES:LANES + rw] = jnp.where(
             (lane_r >= h * rope) & (lane_r < (h + 1) * rope), qr, 0.0).astype(bf16)
-
-    def relay(d, start):
-        src = (sp + n_sp - d) % n_sp
-        if start:
-            rcopy(kvr.at[src, core], kvr.at[src, core], kx_s.at[d], kx_r.at[d], sp, partner).wait_recv()
-            c = rcopy(kvr.at[src, core], kvr.at[src, core], ky_s.at[d], ky_r.at[d], sp, partner)
-            c.start()
-            sends.append(c)
-        else:
-            other = kvr.at[src, 1 - core]
-            rcopy(other, other, ky_s.at[d], ky_r.at[d], sp, partner).wait_recv()
 
     @pl.when(sp < n_sp - 1)
     def _():
@@ -270,10 +340,11 @@
         c = rcopy(stats.at[tp], stats.at[tp], st_s.at[d], st_r.at[d], sp, (tp + d) % n_tp)
         c.start()
         sends.append(c)
-    order = list(range(1, n_sp))
-    for d in order:
-        relay(d, True)
-
+    spread_step(1, "start")
+    other_side(0, "start")
+    for k in range(2, line - 1):
+        spread_step(k, "start")
+        other_side(k - 1, "start")
     for d in range(1, n_tp):
         src = (tp + n_tp - d) % n_tp
         rcopy(stats.at[src], stats.at[src], st_s.at[d], st_r.at[d], sp, partner).wait_recv()
@@ -288,24 +359,40 @@
     loads["woc"].wait()
     cpart[...] = dot(act[...], v_woc[...])
 
-    for d in order:
-        relay(d, False)
-
+    for k in range(max(2, line - 1), line):
+        spread_step(k, "start")
+        other_side(k - 1, "start")
+    other_side(line - 1, "start")
     for name in ("wku", "wvu", "sp"):
         loads[name].wait()
 
-    def expand(s, _):
-        for hf in range(2):
-            lat = kvr[s, hf, 0:half, :]
-            at = pl.ds(pl.multiple_of(s * rows, rows) + hf * half, half)
-            k_all[at, :] = dot(lat, v_wku[...]).astype(bf16)
-            v_all[at, :] = dot(lat, v_wvu[...]).astype(bf16)
-            u = dot(kvr[s, hf, half:half + prow, :], v_sp[...]).astype(bf16)
-            for g in range(groups):
-                r_all[pl.ds(pl.multiple_of(s * rows, rows) + hf * half + g * prow, prow), :] = u[:, g * rw:(g + 1) * rw]
+    def expand(s, hf):
+        lat = kvr[s, hf, 0:half, :]
+        start = pl.multiple_of(s * rows + hf * half, half)
+        k_all[pl.ds(start, half), :] = dot(lat, v_wku[...]).astype(bf16)
+        v_all[pl.ds(start, half), :] = dot(lat, v_wvu[...]).astype(bf16)
+        u = dot(kvr[s, hf, half:half + prow, :], v_sp[...]).astype(bf16)
+        for g in range(groups):
+            r_all[pl.ds(start + g * prow, prow), :] = u[:, g * rw:(g + 1) * rw]
+
+    def expand_all(hf):
+        step = 4 if n_sp % 4 == 0 else 1
+
+        def four(i, _):
+            for j in range(step):
+                expand(i * step + j, hf)
+            return 0
+        lax.fori_loop(0, n_sp // step, four, 0)
+
+    expand_all(core)
+    def relayed(s, _):
+        @pl.when(s != sp)
+        def _():
+            block(s, ky_s, sp, partner, ky_r, 1 - core).wait_recv()
         return 0
 
-    lax.fori_loop(0, n_sp, expand, 0)
+    lax.fori_loop(0, n_sp, relayed, 0)
+    expand_all(1 - core)
 
     keys = n_sp * rows
     nk = keys // kchunk
@@ -315,36 +402,38 @@
     scale2 = float((nope + rope) ** -0.5 * np.log2(np.e))
     lane_v = lax.broadcasted_iota(jnp.int32, (qb, vw), 1)
 
-    def attend(b, hs, result):
-        for h in hs:
-            blk = h // per
-            q = qf[h, b * qb:(b + 1) * qb, :]
-
-            def scores(at):
-                k = jnp.concatenate([k_all[at, blk * LANES:(blk + 1) * LANES], r_all[at, :]], axis=1)
-                return dot_t(q, k)
-
-            if nk == 1:
-                at = slice(0, keys)
+    def attend(b, blk, result):
+        hs = range(blk * per, (blk + 1) * per)
+        q = jnp.concatenate([qf[h, b * qb:(b + 1) * qb, :] for h in hs], axis=0)
+
+        def scores(at):
+            k = jnp.concatenate([k_all[at, blk * LANES:(blk + 1) * LANES], r_all[at, :]], axis=1)
+            return dot_t(q, k)
+
+        if nk == 1:
+            at = slice(0, keys)
+            s = scores(at)
+            m = jnp.max(s, axis=1, keepdims=True)
+            w = jnp.exp2((s - m) * scale2)
+            total = jnp.sum(w, axis=1, keepdims=True)
+            o = dot(w.astype(bf16), v_all[at, :])
+        else:
+            def step(i, carry):
+                m, total, o = carry
+                at = pl.ds(pl.multiple_of(i * kchunk, kchunk), kchunk)
                 s = scores(at)
-                m = jnp.max(s, axis=1, keepdims=True)
-                w = jnp.exp2((s - m) * scale2)
-                total = jnp.sum(w, axis=1, keepdims=True)
-                o = dot(w.astype(bf16), v_all[at, :])
-            else:
-                def step(i, carry):
-                    m, total, o = carry
-                    at = pl.ds(pl.multiple_of(i * kchunk, kchunk), kchunk)
-                    s = scores(at)
-                    nm = jnp.maximum(m, jnp.max(s, axis=1, keepdims=True))
-                    f = jnp.exp2((m - nm) * scale2)
-                    w = jnp.exp2((s - nm) * scale2)
-                    return (nm, total * f + jnp.sum(w, axis=1, keepdims=True),
-                            o * f + dot(w.astype(bf16), v_all[at, :]))
-                m, total, o = lax.fori_loop(0, nk, step, (
-                    jnp.full((qb, 1), -jnp.inf, f32), jnp.zeros((qb, 1), f32), jnp.zeros((qb, vw), f32)))
+                nm = jnp.maximum(m, jnp.max(s, axis=1, keepdims=True))
+                f = jnp.exp2((m - nm) * scale2)
+                w = jnp.exp2((s - nm) * scale2)
+                return (nm, total * f + jnp.sum(w, axis=1, keepdims=True),
+                        o * f + dot(w.astype(bf16), v_all[at, :]))
+            m, total, o = lax.fori_loop(0, nk, step, (
+                jnp.full((per * qb, 1), -jnp.inf, f32), jnp.zeros((per * qb, 1), f32),
+                jnp.zeros((per * qb, vw), f32)))
+        o = o / total
+        for i, h in enumerate(hs):
             mask = (lane_v >= h * vdim) & (lane_v < (h + 1) * vdim)
-            result = jnp.where(mask, o / total, result)
+            result = jnp.where(mask, o[i * qb:(i + 1) * qb], result)
         return result
 
     def partial(b, t, a):
@@ -376,11 +465,15 @@
     zero = jnp.zeros((qb, vw), f32)
     loads["woa"].wait()
     for b in range(rblocks):
-        a = attend(b, range(heads // 2), zero)
-        if b:
-            cross(b - 1)
-        a = attend(b, range(heads // 2, heads), a)
+        a = zero
+        for blk in range(heads // per):
+            a = attend(b, blk, a)
+            if b and blk == 0:
+                cross(b - 1)
         project(b, a.astype(bf16))
+    def done(b):
+        return pltpu.make_async_copy(result.at[b], out.at[pl.ds(b * qb, qb)], out_s.at[b])
+
     cross(rblocks - 1)
     for b in range(rblocks):
         pcopy(b, 0).wait_recv()
@@ -388,12 +481,17 @@
         for j in range(1, pairs):
             ccopy(b, j).wait_recv()
             total = total + from_cross[b, j].astype(f32)
-        out[b * qb:(b + 1) * qb, :] = total.astype(bf16)
+        result[b] = total.astype(bf16)
+        done(b).start()
     for b in range(rblocks):
         for j in range(pairs):
             pcopy(b, j).wait_send()
         for j in range(1, pairs):
             ccopy(b, j).wait_send()
+        done(b).wait()
+    for k in range(line):
+        spread_step(k, "wait_send")
+        other_side(k, "wait_send")
     for c in sends:
         c.wait_send()
 
@@ -427,17 +525,18 @@
     m = np.arange(groups * rw)[None, :]
     spread_mat = jnp.asarray(((l // rope == m // rw) & (l % rope == m % rope)).astype(np.float32), bf16)
     row = lambda v: v.reshape(1, -1)
-    ins = (tokens, row(in_gain), query_down, latent_down, rope_down, row(query_gain), row(latent_gain),
+    rope_t = rope_down.T
+    ins = (tokens, row(in_gain), query_down, latent_down, rope_t, row(query_gain), row(latent_gain),
            query_nope, query_rope, key_up, value_up, conv_value, conv_gate, conv_taps, row(conv_bias),
            row(channel_gain), out_attend, out_conv, *tables, spread_mat)
-    A, V = pl.BlockSpec(memory_space=pl.ANY), pl.BlockSpec(memory_space=pltpu.VMEM)
-    specs = [A, V, A, A, A, V, V, A, A, A, A, A, A, V, V, V, A, A, V, V, V, V, A]
+    specs = [pl.BlockSpec(memory_space=pltpu.HBM)] * len(ins)
     vm = lambda a: pltpu.VMEM(a.shape, a.dtype)
     D = lambda *s: pltpu.SemaphoreType.DMA(s)
     scratch = [
-        pltpu.VMEM((n_tp, rows, dl), bf16), vm(query_down), vm(latent_down), vm(rope_down),
+        pltpu.VMEM((n_tp, rows, dl), bf16), vm(query_down), vm(latent_down), vm(rope_t),
         vm(query_nope), vm(query_rope), vm(key_up), vm(value_up), vm(conv_value), vm(conv_gate),
         vm(out_attend), vm(out_conv), vm(spread_mat),
+        *[vm(ins[i]) for i in (1, 5, 6, 13, 14, 15, 18, 19, 20, 21)],
         pltpu.VMEM((rows, qw), f32), pltpu.VMEM((rows, kvw), f32), pltpu.VMEM((rows, rope), f32),
         pltpu.VMEM((rows, ch), f32), pltpu.VMEM((rows, ch), f32),
         pltpu.VMEM((n_sp, 2, half + prow, kvw), bf16),
@@ -445,24 +544,24 @@
         pltpu.VMEM((keys, rw), bf16), pltpu.VMEM((heads, rows, LANES + rw), bf16),
         pltpu.VMEM((rows + 2 * pad, ch), bf16), pltpu.VMEM((rows + 2 * pad, ch), f32),
         pltpu.VMEM((rows, ch), f32), pltpu.VMEM((n_tp, 8, rows), f32), pltpu.VMEM((rows, ch), bf16),
-        pltpu.VMEM((8, LANES), f32),
         pltpu.VMEM((rows, n_tp * dl), f32),
         pltpu.VMEM((rblocks, pairs, qb, dl), bf16), pltpu.VMEM((rblocks, pairs, qb, dl), bf16),
         pltpu.VMEM((rblocks, pairs, qb, dl), bf16), pltpu.VMEM((rblocks, pairs, qb, dl), bf16),
         pltpu.VMEM((rblocks, pairs, qb, dl), bf16),
-        D(13), D(pairs, tchunks), D(pairs, tchunks), pltpu.SemaphoreType.DMA, pltpu.SemaphoreType.DMA,
-        D(pairs, tchunks), D(pairs, tchunks), D(n_sp), D(n_sp), D(n_sp), D(n_sp),
+        pltpu.VMEM((rblocks, qb, dl), bf16),
+        D(23), D(pairs, tchunks), D(pairs, tchunks), pltpu.SemaphoreType.DMA, pltpu.SemaphoreType.DMA,
+        D(pairs, tchunks), D(pairs, tchunks), *[D(n_sp)] * 6,
         D(2), D(2), D(n_tp), D(n_tp), D(rblocks, pairs), D(rblocks, pairs),
-        D(rblocks, pairs), D(rblocks, pairs),
+        D(rblocks, pairs), D(rblocks, pairs), D(rblocks),
     ]
     return pl.pallas_call(
         functools.partial(body, n_sp, n_tp, rope, nope, heads, tchunks, rblocks, kchunk),
         out_shape=jax.ShapeDtypeStruct((rows, dl), bf16),
         in_specs=specs,
-        out_specs=V,
+        out_specs=pl.BlockSpec(memory_space=pltpu.HBM),
         scratch_shapes=scratch,
         compiler_params=pltpu.CompilerParams(
-            collective_id=0, has_side_effects=True, vmem_limit_bytes=60 * 1024 * 1024),
+            collective_id=0, has_side_effects=True, vmem_limit_bytes=60 << 20),
         name="layer",
     )(*ins)
 

time: 55.8 us -> 46.8 us (0.84)
  the two profiles are of different devices: /device:TPU:12 before, /device:TPU:0 now
where the time goes in v2:
time: 46.8 us; the launch traced here: 46.7 us
  Pallas kernels  45 us (96%)
  local copies, waits for them, and re-layouts  1.67 us (4%)
    pallas_call x1, Pallas kernels, per_device(): pl.pallas_call(functools.partial(body, n_sp, n_tp, rope, nope, heads, tch...  45 us
    unnamed x1, local copies, waits for them, and re-layouts  1.67 us

profile of v2, /device:TPU:0, one launch (start us, length us, event | category | flops | bytes accessed | tf_op | source)
XLA Modules:
  0.0 46.7 jit_solution(2241845057180400110)
XLA Ops:
  0.0 45.0 %layer.1 = bf16[256,512]{1,0:T(8,128)(2,1)} custom-call(bf16[256,512]{1,0:T(8,128)(2,1)} %tok.1, f32[1,2048]{1,0:T(1,128)} %bitcast.7, bf16[2048,512]{1,0:T(8,128)(2,1)} %wq.1, bf16[2048,256]{1,0:T(8,128)(2,1)} %wl.1, bf16[32,2048]{1,0:T(8,128)(2,1)} %bitcast.6, f32[1,512]{1,0:T(1,128)} %bitcast.8, f32[1,256]{1,0:T(1,128)} %bitcast.11, ...), custom_call_target="tpu_custom_call" | custom-call | tf_op jit(solution)/shard_map/layer/pallas_call | solution.py:557
  45.0 1.7 %copy.25 = bf16[256,512]{1,0:T(8,128)(2,1)} copy(bf16[256,512]{1,0:T(8,128)(2,1)} %layer.1) | data formatting | bytes 524288
